TPU v7x, 32 devices: a whole 2x2x4 slice. The times are simulated.
32 devices in a mesh: ra: 8 (over z, y), cb: 4 (over x, core).
Axes of the slice: x: 2, y: 2, z: 4, core: 2. Of those that a mesh axis runs over, the one named last changes fastest.
Arguments:
- tokens: bfloat16 [2048, 4096], P('ra'), may hold values from -16 to 16
- norm_gain: float32 [2, 2048], replicated, may hold values from 0.1 to 1.9
- up_weight: float32 [2, 2048, 6144], P(None, 'ra', 'cb'), may hold values from -0.125 to 0.125
- gate_weight: float32 [2, 2048, 6144], P(None, 'ra', 'cb'), may hold values from -0.125 to 0.125
- up_scale: float32 [2, 6144], P(None, 'cb'), may hold values from 0.5 to 2
- gate_scale: float32 [2, 6144], P(None, 'cb'), may hold values from 0.5 to 2
- up_taps: float32 [2, 3, 6144], P(None, None, 'cb'), may hold values from -3 to 3
- gate_taps: float32 [2, 3, 6144], P(None, None, 'cb'), may hold values from -3 to 3
- down_weight: float32 [2, 2048, 6144], P(None, 'ra', 'cb'), may hold values from -0.078125 to 0.078125
- down_scale: float32 [2, 2048], replicated, may hold values from 0.5 to 2
Outputs:
- mixed: bfloat16 [2048, 4096], P('ra')
All inputs are finite; a program needn't handle non-finite values.
Results may differ from a plain program's by a relative error of at most 0.024.
Values may be sent and summed in bfloat16 or wider, within the bound.
A program may use at most 128 MiB of HBM per device.

v0:
```python
import functools

import jax
import jax.numpy as jnp
from jax import lax
from jax.experimental import pallas as pl
from jax.experimental.pallas import tpu as pltpu
from jax.sharding import PartitionSpec as P

EPS = 1e-06
RESIDUAL = 0.5
MESH = pl.DeviceIdType.MESH


def doublings(low, high):
    bits = []
    while low < high:
        bits.append(low)
        low *= 2
    return bits


def bit_of(value, bit):
    return lax.rem(lax.div(value, bit), 2) if not isinstance(value, int) else (value // bit) % 2


def flip(value, offset):
    for bit in doublings(1, offset + 1):
        if offset & bit:
            value = value + bit - 2 * bit * bit_of(value, bit)
    return value


class Plan:
    def __init__(self, n_ra, n_cb, rows, columns, length, layers, width):
        self.n_ra, self.n_cb, self.rows, self.columns = n_ra, n_cb, rows, columns
        self.length, self.layers, self.width = length, layers, width
        self.n_y = 1 << ((n_ra.bit_length() - 1) // 2)
        self.n_z = n_ra // self.n_y
        self.half = columns // 2
        self.groups = n_ra // 2
        self.group_tokens = length // self.groups
        self.cb_bits = doublings(1, n_cb)
        self.n_steps = len(self.cb_bits) + 1
        self.sizes = [self.group_tokens >> (s + 1) for s in range(self.n_steps)]
        self.own = self.sizes[-1]
        self.q = 1
        while rows * self.q < 256 and self.q < self.n_y:
            self.q *= 2
        self.chunk = rows * self.q
        self.n_chunks = n_ra // self.q
        self.features = n_ra * rows
        cy = self.n_y // self.q
        self.cy = cy
        self.order_bits = [cy] + doublings(2 * cy, self.n_z * cy) + doublings(1, cy)
        self.edge = 8


def kernel(
    p,
    tin,
    up_w,
    gate_w,
    down_w,
    gain,
    up_scale,
    gate_scale,
    up_taps,
    gate_taps,
    down_scale,
    out,
    w,
    give,
    stage,
    st,
    up,
    gate,
    hid,
    tok,
    sq,
    halo,
    obuf,
    ost,
    accs,
    snds,
    rcvs,
    sem,
):
    r, j = lax.axis_index("ra"), lax.axis_index("cb")
    z, y = lax.div(r, p.n_y), lax.rem(r, p.n_y)
    m = lax.rem(z, 2)
    mine = [bit_of(j, bit) for bit in p.cb_bits] + [m]
    n_k = 3 * p.layers

    def group_of(dev):
        return lax.div(lax.div(dev, p.n_y), 2) * p.n_y + lax.rem(dev, p.n_y)

    def sub_row(bits, count):
        start = 0
        for s in range(count):
            start = start + bits[s] * p.sizes[s]
        return start

    def first_token(dev):
        bits = mine[:-1] + [lax.rem(lax.div(dev, p.n_y), 2)]
        return group_of(dev) * p.group_tokens + sub_row(bits, p.n_steps)

    def partner(s):
        if s < p.n_steps - 1:
            return r, flip(j, p.cb_bits[s])
        return flip(r, p.n_y), j

    def copy(src, dst, ssem, rsem, dev):
        return pltpu.make_async_remote_copy(
            src_ref=src,
            dst_ref=dst,
            send_sem=ssem,
            recv_sem=rsem,
            device_id=dev,
            device_id_type=MESH,
        )

    def at_rows(start, size):
        return pl.ds(pl.multiple_of(start, size), size)

    own_row = sub_row(mine, p.n_steps)
    own_rows = at_rows(own_row, p.own)
    my_slab = at_rows(r * p.rows, p.rows)

    barrier = pltpu.get_barrier_semaphore()
    for off in range(1, p.n_ra):
        pl.semaphore_signal(barrier, inc=1, device_id=(flip(r, off), j), device_id_type=MESH)
    for bit in p.cb_bits:
        pl.semaphore_signal(barrier, inc=1, device_id=(r, flip(j, bit)), device_id_type=MESH)

    def load(k):
        layer, kind = k // 3, k % 3
        source = (up_w, gate_w, down_w)[kind]
        return pltpu.make_async_copy(source.at[layer], stage.at[k % 2], sem["stage"].at[k % 2])

    load(0).start()
    load(1).start()
    own_tokens = pltpu.make_async_copy(
        tin.at[at_rows(first_token(r), p.own)], tok.at[r], sem["local"].at[0]
    )
    own_tokens.start()
    pl.semaphore_wait(barrier, p.n_ra - 1 + len(p.cb_bits))

    def token_send(off):
        dev = flip(r, off)
        return copy(
            tin.at[at_rows(first_token(dev), p.own)],
            tok.at[r],
            sem["tok_s"].at[off],
            sem["tok_r"].at[r],
            (dev, j),
        )

    for off in range(1, p.n_ra):
        token_send(off).start()

    def slab(k, dev):
        return w.at[k, at_rows(dev * p.rows, p.rows)]

    def z_send(k, dz):
        source = give.at[k] if dz % 2 else slab(k, r)
        return copy(
            source, slab(k, r), sem["z"].at[k, dz], sem["w"].at[k, r], (flip(z, dz) * p.n_y + y, j)
        )

    def y_send(k, dz, dy):
        dev = flip(z, dz) * p.n_y + y
        return copy(
            slab(k, dev),
            slab(k, dev),
            sem["y"].at[k, dz, dy],
            sem["w"].at[k, dev],
            (z * p.n_y + flip(y, dy), j),
        )

    def slab_wait(k, dev):
        copy(slab(k, dev), slab(k, dev), sem["z"].at[k, 0], sem["w"].at[k, dev], (r, j)).wait_recv()

    def forward(k, dz):
        if dz:
            slab_wait(k, flip(z, dz) * p.n_y + y)
        for dy in range(1, p.n_y):
            y_send(k, dz, dy).start()

    def convert(k):
        load(k).wait()
        tile = min(64, p.rows)

        @pl.loop(0, p.rows // tile)
        def _(t):
            rows = at_rows(t * tile, tile)
            keep = stage[k % 2, rows, pl.ds(pl.multiple_of(m * p.half, 128), p.half)]
            rest = stage[k % 2, rows, pl.ds(pl.multiple_of((1 - m) * p.half, 128), p.half)]
            w[k, at_rows(r * p.rows + t * tile, tile), :] = keep.astype(jnp.bfloat16)
            give[k, rows, :] = rest.astype(jnp.bfloat16)

        if k + 2 < n_k:
            load(k + 2).start()

    far = list(range(2, p.n_z))

    def first_sends(k):
        z_send(k, 1).start()
        if k < 2:
            for dy in range(1, p.n_y):
                y_send(k, 0, dy).start()
        if 1 <= k <= 3:
            for dz in far:
                z_send(k - 1, dz).start()

    convert(0)

    own_tokens.wait()
    for src in range(p.n_ra):
        lanes = slice(src * p.rows, (src + 1) * p.rows)

        @pl.when(r != src)
        def _():
            copy(
                tok.at[src], tok.at[src], sem["tok_s"].at[0], sem["tok_r"].at[src], (r, j)
            ).wait_recv()

        st[0, own_rows, lanes] = tok[src]

    def block_rows(a):
        count = p.n_steps - a
        size = p.own << a
        return sub_row(mine, count), size

    def gather_copy(layer, a, lanes, ssem, rsem):
        start, size = block_rows(a)
        ref = st.at[layer, at_rows(start, size), lanes]
        return copy(ref, ref, ssem, rsem, partner(p.n_steps - 1 - a))

    def gather_wait(layer, a, lanes, ssem, rsem):
        start, size = block_rows(a)
        s = p.n_steps - 1 - a
        ref = st.at[layer, at_rows(start + (1 - 2 * mine[s]) * size, size), lanes]
        copy(ref, ref, ssem, rsem, (r, j)).wait_recv()

    everything = pl.ds(0, p.features)

    def gather0(a):
        return gather_copy(0, a, everything, sem["g0_s"].at[a], sem["g0_r"].at[a])

    def gather0_wait(a):
        gather_wait(0, a, everything, sem["g0_s"].at[a], sem["g0_r"].at[a])

    convert(1)
    gather0(0).start()
    for k in range(2, n_k):
        first_sends(k - 2)
        convert(k)
    first_sends(n_k - 2)
    first_sends(n_k - 1)

    for a in range(p.n_steps):
        gather0_wait(a)
        if a + 1 < p.n_steps:
            gather0(a + 1).start()
        if a < 2:
            forward(a, 1)

    def chunk_of(i):
        base = (z - m) * p.cy + lax.div(y, p.q)
        total = 0
        shift = 1
        for bit in p.order_bits:
            total = total + lax.rem(lax.div(base, bit) + lax.div(i, shift), 2) * bit
            shift *= 2
        return total

    def chunk_lanes(f):
        return pl.ds(pl.multiple_of(f * p.chunk, p.chunk), p.chunk)

    def chunk_wait(k, f):
        for t in range(p.q):
            dev = f * p.q + t

            @pl.when(lax.rem(dev, p.n_y) != y)
            def _():
                slab_wait(k, dev)

    tile = min(256, p.group_tokens)
    fine = 64

    def squares(layer, lanes, first):
        @pl.loop(0, p.group_tokens // fine)
        def _(t):
            rows = at_rows(t * fine, fine)
            values = st[layer, rows, lanes].astype(jnp.float32)
            total = None
            for c in range(p.chunk // 128):
                part = values[:, c * 128 : (c + 1) * 128]
                total = part * part if total is None else total + part * part
            if first is None:
                sq[rows, :] = sq[rows, :] + total
            else:

                @pl.when(first)
                def _():
                    sq[rows, :] = total

                @pl.when(jnp.logical_not(first))
                def _():
                    sq[rows, :] = sq[rows, :] + total

    @pl.loop(0, p.n_chunks)
    def _(i):
        squares(0, chunk_lanes(i), i == 0)

    def product(layer, k, dst):
        @pl.loop(0, p.n_chunks)
        def _(i):
            f = chunk_of(i)
            chunk_wait(k, f)
            lanes = chunk_lanes(f)
            weights = w.at[k, at_rows(f * p.chunk, p.chunk)]

            @pl.loop(0, p.group_tokens // tile)
            def _(t):
                rows = at_rows(t * tile, tile)
                scaled = st[layer, rows, lanes].astype(jnp.float32) * gain[layer : layer + 1, lanes]
                term = jnp.dot(
                    scaled.astype(jnp.bfloat16), weights[...], preferred_element_type=jnp.float32
                )
                to = pl.ds(pl.multiple_of(p.edge + t * tile, 8), tile)

                @pl.when(i == 0)
                def _():
                    dst[to, :] = term

                @pl.when(i > 0)
                def _():
                    dst[to, :] = dst[to, :] + term

    own_half = pl.ds(pl.multiple_of(m * p.half, 128), p.half)
    group = group_of(r)
    following = group + 1
    following_dev = (lax.div(following, p.n_y) * 2 + m) * p.n_y + lax.rem(following, p.n_y)

    def halo_copy(layer, which):
        source = (up, gate)[which]
        return copy(
            source.at[pl.ds(p.group_tokens, p.edge)],
            halo.at[layer, which],
            sem["h_s"].at[layer, which],
            sem["h_r"].at[layer, which],
            (following_dev, j),
        )

    def convolve(layer):
        scale_u = up_scale[layer : layer + 1, own_half]
        scale_g = gate_scale[layer : layer + 1, own_half]

        @pl.loop(0, p.group_tokens // fine)
        def _(t):
            total = jnp.sum(sq[at_rows(t * fine, fine), :], axis=1, keepdims=True)
            inverse = lax.rsqrt(total * (1.0 / p.features) + EPS)
            rows = pl.ds(pl.multiple_of(p.edge + t * fine, 8), fine)
            up[rows, :] = up[rows, :] * inverse * scale_u
            gate[rows, :] = gate[rows, :] * inverse * scale_g

        @pl.when(following < p.groups)
        def _():
            halo_copy(layer, 0).start()
            halo_copy(layer, 1).start()

        @pl.when(group > 0)
        def _():
            for which, dst in ((0, up), (1, gate)):
                copy(
                    halo.at[layer, which],
                    halo.at[layer, which],
                    sem["h_s"].at[layer, which],
                    sem["h_r"].at[layer, which],
                    (r, j),
                ).wait_recv()
                dst[0 : p.edge, :] = halo[layer, which]

        @pl.when(group == 0)
        def _():
            up[0 : p.edge, :] = jnp.zeros((p.edge, p.half), jnp.float32)
            gate[0 : p.edge, :] = jnp.zeros((p.edge, p.half), jnp.float32)

        taps_u = up_taps[layer, :, own_half]
        taps_g = gate_taps[layer, :, own_half]

        def taps_over(ref, taps, t):
            values = ref[pl.ds(pl.multiple_of(t * fine, 8), fine + p.edge), :]
            low = p.edge + 1 - p.width
            total = taps[0:1] * values[low : low + fine]
            for c in range(1, p.width):
                total = total + taps[c : c + 1] * values[low + c : low + c + fine]
            return total

        @pl.loop(0, p.group_tokens // fine)
        def _(t):
            conv_gate = taps_over(gate, taps_g, t)
            conv_up = taps_over(up, taps_u, t)
            value = conv_gate / (1.0 + jnp.exp(-conv_gate)) * conv_up
            hid[at_rows(t * fine, fine), :] = value.astype(jnp.bfloat16)

    def reduce_copy(layer, s, i):
        return copy(
            snds[s].at[i],
            rcvs[s].at[layer, i],
            sem["r_s"].at[layer, s, i],
            sem["r_r"].at[layer, s, i],
            partner(s),
        )

    def reduce_wait(layer, s, i):
        ref = rcvs[s].at[layer, i]
        copy(ref, ref, sem["r_s"].at[layer, s, i], sem["r_r"].at[layer, s, i], (r, j)).wait_recv()

    def down_stage(layer, i):
        k = 3 * layer + 2
        f = chunk_of(i)
        chunk_wait(k, f)
        weights = w.at[k, at_rows(f * p.chunk, p.chunk)]
        size = p.sizes[0]
        step = min(tile, size)

        def term(start):
            return lax.dot_general(
                hid[pl.ds(pl.multiple_of(start, step), step), :],
                weights[...],
                (((1,), (1,)), ((), ())),
                preferred_element_type=jnp.float32,
            )

        @pl.loop(0, size // step)
        def _(t):
            rows = at_rows(t * step, step)
            snds[0][i, rows, :] = term((1 - mine[0]) * size + t * step).astype(jnp.bfloat16)

        @pl.loop(0, size // step)
        def _(t):
            accs[0][at_rows(t * step, step), :] = term(mine[0] * size + t * step)

        reduce_copy(layer, 0, i).start()

    def reduce_stage(layer, s, i):
        reduce_wait(layer, s - 1, i)
        size = p.sizes[s]
        give_rows = at_rows((1 - mine[s]) * size, size)
        keep_rows = at_rows(mine[s] * size, size)
        arrived = rcvs[s - 1][layer, i, give_rows, :].astype(jnp.float32)
        snds[s][i] = (accs[s - 1][give_rows, :] + arrived).astype(jnp.bfloat16)
        arrived = rcvs[s - 1][layer, i, keep_rows, :].astype(jnp.float32)
        accs[s][...] = accs[s - 1][keep_rows, :] + arrived
        reduce_copy(layer, s, i).start()

    def gather1(a, f):
        return gather_copy(1, a, chunk_lanes(f), sem["g_s"].at[a, f], sem["g_r"].at[a, f])

    def gather1_wait(a, f):
        gather_wait(1, a, chunk_lanes(f), sem["g_s"].at[a, f], sem["g_r"].at[a, f])

    def out_copy(f, t):
        return copy(
            ost.at[f, t],
            obuf.at[at_rows(first_token(r), p.own)],
            sem["o_s"].at[f, t],
            sem["o_r"].at[r],
            (f * p.q + t, j),
        )

    def last_stage(layer, i):
        f = chunk_of(i)
        s = p.n_steps - 1
        reduce_wait(layer, s, i)
        lanes = chunk_lanes(f)
        total = accs[s][...] + rcvs[s][layer, i].astype(jnp.float32)
        before = st[layer, own_rows, lanes].astype(jnp.float32)
        value = total * down_scale[layer : layer + 1, lanes] + RESIDUAL * before
        value = value.astype(jnp.bfloat16)
        if layer + 1 < p.layers:
            st[layer + 1, own_rows, lanes] = value
            gather1(0, f).start()
        else:
            for t in range(p.q):
                ost[f, t] = value[:, t * p.rows : (t + 1) * p.rows]
                dev = f * p.q + t

                @pl.when(dev == r)
                def _():
                    obuf[at_rows(first_token(r), p.own), :] = ost[f, t]

                @pl.when(dev != r)
                def _():
                    out_copy(f, t).start()

    def gather_stage(a, i):
        f = chunk_of(i)
        gather1_wait(a, f)
        if a + 1 < p.n_steps:
            gather1(a + 1, f).start()
        else:
            squares(1, chunk_lanes(f), i == 0)

    def pipeline(stages, tasks):
        count = p.n_chunks + len(stages) - 1

        @pl.loop(0, count)
        def _(it):
            for back in reversed(range(len(stages))):
                i = it - back

                @pl.when(jnp.logical_and(i >= 0, i < p.n_chunks))
                def _():
                    stages[back](i)

            for index, task in enumerate(tasks):

                @pl.when(it == 1 + index * (count - 2) // len(tasks))
                def _():
                    task()

    def pump(k):
        for dz in far:
            forward(k, dz)
        if k + 2 < n_k:
            forward(k + 2, 0)
            forward(k + 2, 1)

    for layer in range(p.layers):
        last = layer + 1 == p.layers
        k = 3 * layer
        if layer:
            for dz in far:
                z_send(k + 2, dz).start()
        pump(k)
        product(layer, k, up)
        pump(k + 1)
        product(layer, k + 1, gate)
        convolve(layer)
        pump(k + 2)
        stages = [functools.partial(down_stage, layer)]
        stages += [functools.partial(reduce_stage, layer, s) for s in range(1, p.n_steps)]
        stages += [functools.partial(last_stage, layer)]
        tasks = []
        if not last:
            stages += [functools.partial(gather_stage, a) for a in range(p.n_steps)]
            tasks = [
                lambda k=k, dz=dz: z_send(k, dz).start() for k in (k + 3, k + 4) for dz in far
            ]
        pipeline(stages, tasks)

        @pl.loop(0, p.n_chunks)
        def _(i):
            for s in range(p.n_steps):
                reduce_copy(layer, s, i).wait_send()

        @pl.when(following < p.groups)
        def _():
            halo_copy(layer, 0).wait_send()
            halo_copy(layer, 1).wait_send()

    sources = [
        (pz, py)
        for py in range(p.n_y)
        for pz in range(0, p.n_z, 2)
    ]
    n_out = p.n_steps - 1

    def out_rows(index, a, flipped):
        pz, py = sources[index]
        dev = flip(z, pz) * p.n_y + flip(y, py)
        start, size = block_rows(a)
        if flipped:
            start = start + (1 - 2 * mine[p.n_steps - 1 - a]) * size
        return obuf.at[at_rows(group_of(dev) * p.group_tokens + start, size)]

    def out_gather(index, a):
        ref = out_rows(index, a, False)
        return copy(
            ref,
            ref,
            sem["oa_s"].at[a - 1, index],
            sem["oa_r"].at[a - 1, index],
            partner(p.n_steps - 1 - a),
        )

    for index, (pz, py) in enumerate(sources):
        for low in range(2):
            dev = flip(z - m + low, pz) * p.n_y + flip(y, py)

            @pl.when(dev != r)
            def _():
                ref = obuf.at[at_rows(first_token(dev), p.own)]
                copy(ref, ref, sem["o_s"].at[0, 0], sem["o_r"].at[dev], (r, j)).wait_recv()

        out_gather(index, 1).start()
    for a in range(1, p.n_steps):
        for index in range(len(sources)):
            ref = out_rows(index, a, True)
            copy(
                ref, ref, sem["oa_s"].at[a - 1, index], sem["oa_r"].at[a - 1, index], (r, j)
            ).wait_recv()
            if a + 1 < p.n_steps:
                out_gather(index, a + 1).start()

    result = pltpu.make_async_copy(obuf, out, sem["local"].at[0])
    result.start()
    for off in range(1, p.n_ra):
        token_send(off).wait_send()
    for k in range(n_k):
        for dz in range(1, p.n_z):
            z_send(k, dz).wait_send()
        for dz in range(p.n_z):
            for dy in range(1, p.n_y):
                y_send(k, dz, dy).wait_send()
    for a in range(p.n_steps):
        gather0(a).wait_send()

    @pl.loop(0, p.n_chunks)
    def _(f):
        for a in range(p.n_steps):
            gather1(a, f).wait_send()
        for t in range(p.q):

            @pl.when(f * p.q + t != r)
            def _():
                out_copy(f, t).wait_send()

    for a in range(1, p.n_steps):
        for index in range(len(sources)):
            out_gather(index, a).wait_send()
    result.wait()


def per_device(
    tokens,
    norm_gain,
    up_weight,
    gate_weight,
    up_scale,
    gate_scale,
    up_taps,
    gate_taps,
    down_weight,
    down_scale,
):
    layers, rows, columns = up_weight.shape
    p = Plan(
        lax.axis_size("ra"),
        lax.axis_size("cb"),
        rows,
        columns,
        tokens.shape[1],
        layers,
        up_taps.shape[1],
    )
    n_k = 3 * layers
    bf16, f32 = jnp.bfloat16, jnp.float32
    dma = pltpu.SemaphoreType.DMA
    in_hbm = pl.BlockSpec(memory_space=pl.ANY)
    in_vmem = pl.BlockSpec(memory_space=pltpu.VMEM)
    sems = {
        "stage": dma((2,)),
        "local": dma((1,)),
        "tok_s": dma((p.n_ra,)),
        "tok_r": dma((p.n_ra,)),
        "w": dma((n_k, p.n_ra)),
        "z": dma((n_k, p.n_z)),
        "y": dma((n_k, p.n_z, p.n_y)),
        "g0_s": dma((p.n_steps,)),
        "g0_r": dma((p.n_steps,)),
        "g_s": dma((p.n_steps, p.n_chunks)),
        "g_r": dma((p.n_steps, p.n_chunks)),
        "r_s": dma((layers, p.n_steps, p.n_chunks)),
        "r_r": dma((layers, p.n_steps, p.n_chunks)),
        "h_s": dma((layers, 2)),
        "h_r": dma((layers, 2)),
        "o_s": dma((p.n_chunks, p.q)),
        "o_r": dma((p.n_ra,)),
        "oa_s": dma((p.n_steps - 1, p.groups)),
        "oa_r": dma((p.n_steps - 1, p.groups)),
    }
    names = list(sems)
    n_s = p.n_steps

    def body(*refs):
        head, rest = refs[:11 + 12], refs[11 + 12 :]
        accs, snds, rcvs = rest[:n_s], rest[n_s : 2 * n_s], rest[2 * n_s : 3 * n_s]
        kernel(p, *head, accs, snds, rcvs, dict(zip(names, rest[3 * n_s :])))

    turned = pl.pallas_call(
        body,
        out_shape=jax.ShapeDtypeStruct((p.length, rows), bf16),
        in_specs=[in_hbm] * 4 + [in_vmem] * 6,
        out_specs=in_hbm,
        scratch_shapes=[
            pltpu.VMEM((n_k, p.features, p.half), bf16),
            pltpu.VMEM((n_k, rows, p.half), bf16),
            pltpu.VMEM((2, rows, columns), f32),
            pltpu.VMEM((layers, p.group_tokens, p.features), bf16),
            pltpu.VMEM((p.edge + p.group_tokens, p.half), f32),
            pltpu.VMEM((p.edge + p.group_tokens, p.half), f32),
            pltpu.VMEM((p.group_tokens, p.half), bf16),
            pltpu.VMEM((p.n_ra, p.own, rows), bf16),
            pltpu.VMEM((p.group_tokens, 128), f32),
            pltpu.VMEM((layers, 2, p.edge, p.half), f32),
            pltpu.VMEM((p.length, rows), bf16),
            pltpu.VMEM((p.n_chunks, p.q, p.own, rows), bf16),
        ]
        + [pltpu.VMEM((size, p.chunk), f32) for size in p.sizes]
        + [pltpu.VMEM((p.n_chunks, size, p.chunk), bf16) for size in p.sizes]
        + [pltpu.VMEM((layers, p.n_chunks, size, p.chunk), bf16) for size in p.sizes]
        + [sems[name] for name in names],
        compiler_params=pltpu.CompilerParams(
            collective_id=0, has_side_effects=True, vmem_limit_bytes=66 * 1000 * 1000
        ),
        name="layers",
    )(
        tokens.T,
        up_weight,
        gate_weight,
        down_weight,
        norm_gain,
        up_scale,
        gate_scale,
        up_taps,
        gate_taps,
        down_scale,
    )
    return turned.T


def solution(mesh):
    placed = (
        P("ra", None),
        P(),
        P(None, "ra", "cb"),
        P(None, "ra", "cb"),
        P(None, "cb"),
        P(None, "cb"),
        P(None, None, "cb"),
        P(None, None, "cb"),
        P(None, "ra", "cb"),
        P(),
    )
    return jax.shard_map(
        per_device, mesh=mesh, in_specs=placed, out_specs=P("ra", None), check_vma=False
    )
```

profile of v0, /device:TPU:17, one launch (start us, length us, event | category | flops | bytes accessed | tf_op | source)
XLA Modules:
  0.0 369.7 jit_solution(94592278355003713)
XLA Ops:
  0.0 1.4 copy.12.refs_7_
  1.4 1.4 copy.13.refs_8_
  2.8 4.1 %copy.11 = bf16[256,4096]{0,1:T(8,128)(2,1)} copy(bf16[256,4096]{1,0:T(8,128)(2,1)} %param.10) | data formatting | bytes 4194304 | tf_op args[0]
  6.9 358.7 %layers.1 = bf16[4096,256]{1,0:T(8,128)(2,1)} custom-call(bf16[4096,256]{1,0:T(8,128)(2,1)} %bitcast.3, f32[2,256,1536]{2,1,0:T(8,128)} %refs_1_.1, f32[2,256,1536]{2,1,0:T(8,128)} %refs_2_.1, f32[2,256,1536]{2,1,0:T(8,128)} %refs_3_.1, f32[2,2048]{1,0:T(2,128)} %refs_4_.1, f32[2,1536]{1,0:T(2,128)} %refs_5_.1, f32[2,1536]{1,0:T(2,128)} %refs_6_.1, ...), custom_call_target="tpu_custom_call" | custom-call | tf_op jit(solution)/shard_map/layers/pallas_call | solution.py:695
  365.6 4.1 %copy.14 = bf16[256,4096]{1,0:T(8,128)(2,1)} copy(bf16[256,4096]{0,1:T(8,128)(2,1)} %bitcast.2) | data formatting | bytes 4194304 | tf_op jit(solution)/shard_map/transpose | solution.py:734
where the time goes:
time: 370 us
  Pallas kernels  359 us (97%)
  local copies, waits for them, and re-layouts  10.9 us (3%)
    pallas_call x1, Pallas kernels, per_device(): pl.pallas_call(body, out_shape=jax.ShapeDtypeStruct((p.length, rows), bf1...  359 us

commit v1 on v0

--- a/solution.py
+++ b/solution.py
@@ -52,8 +52,10 @@
         self.features = n_ra * rows
         cy = self.n_y // self.q
         self.cy = cy
-        self.order_bits = [cy] + doublings(2 * cy, self.n_z * cy) + doublings(1, cy)
+        self.order_bits = [cy] + doublings(1, cy) + doublings(2 * cy, self.n_z * cy)
         self.edge = 8
+        self.extra = 16
+        self.slots = 3
 
 
 def kernel(
@@ -77,6 +79,11 @@
     gate,
     hid,
     tok,
+    tok_e,
+    st_e,
+    up_e,
+    gate_e,
+    sq_e,
     sq,
     halo,
     obuf,
@@ -144,7 +151,16 @@
         tin.at[at_rows(first_token(r), p.own)], tok.at[r], sem["local"].at[0]
     )
     own_tokens.start()
-    pl.semaphore_wait(barrier, p.n_ra - 1 + len(p.cb_bits))
+    group = group_of(r)
+
+    def extra_rows(dev):
+        return at_rows(group_of(dev) * p.group_tokens - p.extra, p.extra)
+
+    own_extra = pltpu.make_async_copy(tin.at[extra_rows(r)], tok_e.at[r], sem["local"].at[1])
+
+    @pl.when(group > 0)
+    def _():
+        own_extra.start()
 
     def token_send(off):
         dev = flip(r, off)
@@ -156,8 +172,16 @@
             (dev, j),
         )
 
-    for off in range(1, p.n_ra):
-        token_send(off).start()
+
+    def extra_send(off):
+        dev = flip(r, off)
+        return copy(
+            tin.at[extra_rows(dev)],
+            tok_e.at[r],
+            sem["toke_s"].at[off],
+            sem["toke_r"].at[r],
+            (dev, j),
+        )
 
     def slab(k, dev):
         return w.at[k, at_rows(dev * p.rows, p.rows)]
@@ -204,28 +228,18 @@
 
     far = list(range(2, p.n_z))
 
-    def first_sends(k):
-        z_send(k, 1).start()
-        if k < 2:
-            for dy in range(1, p.n_y):
-                y_send(k, 0, dy).start()
-        if 1 <= k <= 3:
+    def is_inner(plane):
+        return jnp.logical_and(plane > 0, plane < p.n_z - 1)
+
+    def far_send(k):
+        for wanted in (True, False):
             for dz in far:
-                z_send(k - 1, dz).start()
-
-    convert(0)
-
-    own_tokens.wait()
-    for src in range(p.n_ra):
-        lanes = slice(src * p.rows, (src + 1) * p.rows)
-
-        @pl.when(r != src)
-        def _():
-            copy(
-                tok.at[src], tok.at[src], sem["tok_s"].at[0], sem["tok_r"].at[src], (r, j)
-            ).wait_recv()
-
-        st[0, own_rows, lanes] = tok[src]
+
+                @pl.when(is_inner(flip(z, dz)) == wanted)
+                def _():
+                    z_send(k, dz).start()
+
+    inner = is_inner(z)
 
     def block_rows(a):
         count = p.n_steps - a
@@ -251,20 +265,80 @@
     def gather0_wait(a):
         gather_wait(0, a, everything, sem["g0_s"].at[a], sem["g0_r"].at[a])
 
+    convert(0)
     convert(1)
+    with jax.named_scope("barrier"):
+        pl.semaphore_wait(barrier, p.n_ra - 1 + len(p.cb_bits))
+    for off in range(1, p.n_ra):
+        token_send(off).start()
+
+        @pl.when(group_of(flip(r, off)) > 0)
+        def _():
+            extra_send(off).start()
+
+    forward(0, 0)
+    forward(1, 0)
+    convert(2)
+    with jax.named_scope("tokens"):
+        own_tokens.wait()
+        for src in range(p.n_ra):
+            lanes = slice(src * p.rows, (src + 1) * p.rows)
+
+            @pl.when(r != src)
+            def _():
+                copy(
+                    tok.at[src], tok.at[src], sem["tok_s"].at[0], sem["tok_r"].at[src], (r, j)
+                ).wait_recv()
+
+            st[0, own_rows, lanes] = tok[src]
+
+    convert(3)
     gather0(0).start()
-    for k in range(2, n_k):
-        first_sends(k - 2)
-        convert(k)
-    first_sends(n_k - 2)
-    first_sends(n_k - 1)
-
+    z_send(0, 1).start()
+    z_send(1, 1).start()
+
+    @pl.when(group > 0)
+    def _():
+        own_extra.wait()
+        for src in range(p.n_ra):
+
+            @pl.when(r != src)
+            def _():
+                copy(
+                    tok_e.at[src], tok_e.at[src], sem["toke_s"].at[0], sem["toke_r"].at[src], (r, j)
+                ).wait_recv()
+
+            st_e[:, src * p.rows : (src + 1) * p.rows] = tok_e[src]
+        values = st_e[...].astype(jnp.float32)
+        total = None
+        for c in range(p.features // 128):
+            part = values[:, c * 128 : (c + 1) * 128]
+            total = part * part if total is None else total + part * part
+        sq_e[...] = total
+
+    far_send(0)
+    forward(2, 0)
+    convert(4)
+    convert(5)
     for a in range(p.n_steps):
-        gather0_wait(a)
+        with jax.named_scope(f"gather0#a={a}"):
+            gather0_wait(a)
         if a + 1 < p.n_steps:
             gather0(a + 1).start()
+        if a == 0:
+            far_send(1)
+            z_send(2, 1).start()
+            z_send(3, 1).start()
+        if a == 1:
+            far_send(2)
+            z_send(4, 1).start()
+            z_send(5, 1).start()
         if a < 2:
-            forward(a, 1)
+            with jax.named_scope(f"near#k={a}"):
+                forward(a, 1)
+        if a == 1:
+            for dz in far:
+                forward(0, dz)
 
     def chunk_of(i):
         base = (z - m) * p.cy + lax.div(y, p.q)
@@ -314,33 +388,50 @@
     def _(i):
         squares(0, chunk_lanes(i), i == 0)
 
-    def product(layer, k, dst):
-        @pl.loop(0, p.n_chunks)
-        def _(i):
-            f = chunk_of(i)
-            chunk_wait(k, f)
-            lanes = chunk_lanes(f)
-            weights = w.at[k, at_rows(f * p.chunk, p.chunk)]
-
-            @pl.loop(0, p.group_tokens // tile)
-            def _(t):
-                rows = at_rows(t * tile, tile)
-                scaled = st[layer, rows, lanes].astype(jnp.float32) * gain[layer : layer + 1, lanes]
+    def product_chunk(layer, k, dst, i, first):
+        f = chunk_of(i)
+        chunk_wait(k, f)
+        lanes = chunk_lanes(f)
+        weights = w.at[k, at_rows(f * p.chunk, p.chunk)]
+
+        @pl.loop(0, p.group_tokens // tile)
+        def _(t):
+            rows = at_rows(t * tile, tile)
+            scaled = st[layer, rows, lanes].astype(jnp.float32) * gain[layer : layer + 1, lanes]
+            term = jnp.dot(
+                scaled.astype(jnp.bfloat16), weights[...], preferred_element_type=jnp.float32
+            )
+            to = pl.ds(pl.multiple_of(p.edge + t * tile, 8), tile)
+            dst[to, :] = term if first else dst[to, :] + term
+
+        if layer == 0:
+
+            @pl.when(group > 0)
+            def _():
+                scaled = st_e[:, lanes].astype(jnp.float32) * gain[layer : layer + 1, lanes]
                 term = jnp.dot(
                     scaled.astype(jnp.bfloat16), weights[...], preferred_element_type=jnp.float32
                 )
-                to = pl.ds(pl.multiple_of(p.edge + t * tile, 8), tile)
-
-                @pl.when(i == 0)
-                def _():
-                    dst[to, :] = term
-
-                @pl.when(i > 0)
-                def _():
-                    dst[to, :] = dst[to, :] + term
+                to = (up_e, gate_e)[k % 3]
+                to[...] = term if first else to[...] + term
+
+    def product(layer, k, dst):
+        product_chunk(layer, k, dst, 0, True)
+
+        @pl.loop(1, p.n_chunks)
+        def _(i):
+            product_chunk(layer, k, dst, i, False)
+
+    def product_stage(layer, k, dst, i):
+        @pl.when(i == 0)
+        def _():
+            product_chunk(layer, k, dst, i, True)
+
+        @pl.when(i > 0)
+        def _():
+            product_chunk(layer, k, dst, i, False)
 
     own_half = pl.ds(pl.multiple_of(m * p.half, 128), p.half)
-    group = group_of(r)
     following = group + 1
     following_dev = (lax.div(following, p.n_y) * 2 + m) * p.n_y + lax.rem(following, p.n_y)
 
@@ -354,7 +445,7 @@
             (following_dev, j),
         )
 
-    def convolve(layer):
+    def convolve(layer, between=None):
         scale_u = up_scale[layer : layer + 1, own_half]
         scale_g = gate_scale[layer : layer + 1, own_half]
 
@@ -366,30 +457,42 @@
             up[rows, :] = up[rows, :] * inverse * scale_u
             gate[rows, :] = gate[rows, :] * inverse * scale_g
 
-        @pl.when(following < p.groups)
-        def _():
-            halo_copy(layer, 0).start()
-            halo_copy(layer, 1).start()
+        if layer:
+
+            @pl.when(following < p.groups)
+            def _():
+                halo_copy(layer, 0).start()
+                halo_copy(layer, 1).start()
+
+            between()
 
         @pl.when(group > 0)
         def _():
-            for which, dst in ((0, up), (1, gate)):
-                copy(
-                    halo.at[layer, which],
-                    halo.at[layer, which],
-                    sem["h_s"].at[layer, which],
-                    sem["h_r"].at[layer, which],
-                    (r, j),
-                ).wait_recv()
-                dst[0 : p.edge, :] = halo[layer, which]
+            if layer:
+                for which, dst in ((0, up), (1, gate)):
+                    copy(
+                        halo.at[layer, which],
+                        halo.at[layer, which],
+                        sem["h_s"].at[layer, which],
+                        sem["h_r"].at[layer, which],
+                        (r, j),
+                    ).wait_recv()
+                    dst[0 : p.edge, :] = halo[layer, which]
+            else:
+                total = jnp.sum(sq_e[...], axis=1, keepdims=True)
+                inverse = lax.rsqrt(total * (1.0 / p.features) + EPS)
+                up_values = up_e[...] * inverse * scale_u
+                gate_values = gate_e[...] * inverse * scale_g
+                up[0 : p.edge, :] = up_values[p.extra - p.edge :]
+                gate[0 : p.edge, :] = gate_values[p.extra - p.edge :]
 
         @pl.when(group == 0)
         def _():
             up[0 : p.edge, :] = jnp.zeros((p.edge, p.half), jnp.float32)
             gate[0 : p.edge, :] = jnp.zeros((p.edge, p.half), jnp.float32)
 
-        taps_u = up_taps[layer, :, own_half]
-        taps_g = gate_taps[layer, :, own_half]
+        taps_u = up_taps[:, layer, own_half]
+        taps_g = gate_taps[:, layer, own_half]
 
         def taps_over(ref, taps, t):
             values = ref[pl.ds(pl.multiple_of(t * fine, 8), fine + p.edge), :]
@@ -442,7 +545,7 @@
 
         @pl.loop(0, size // step)
         def _(t):
-            accs[0][at_rows(t * step, step), :] = term(mine[0] * size + t * step)
+            accs[0][lax.rem(i, p.slots), at_rows(t * step, step), :] = term(mine[0] * size + t * step)
 
         reduce_copy(layer, 0, i).start()
 
@@ -452,9 +555,10 @@
         give_rows = at_rows((1 - mine[s]) * size, size)
         keep_rows = at_rows(mine[s] * size, size)
         arrived = rcvs[s - 1][layer, i, give_rows, :].astype(jnp.float32)
-        snds[s][i] = (accs[s - 1][give_rows, :] + arrived).astype(jnp.bfloat16)
+        slot = lax.rem(i, p.slots)
+        snds[s][i] = (accs[s - 1][slot, give_rows, :] + arrived).astype(jnp.bfloat16)
         arrived = rcvs[s - 1][layer, i, keep_rows, :].astype(jnp.float32)
-        accs[s][...] = accs[s - 1][keep_rows, :] + arrived
+        accs[s][slot] = accs[s - 1][slot, keep_rows, :] + arrived
         reduce_copy(layer, s, i).start()
 
     def gather1(a, f):
@@ -477,7 +581,7 @@
         s = p.n_steps - 1
         reduce_wait(layer, s, i)
         lanes = chunk_lanes(f)
-        total = accs[s][...] + rcvs[s][layer, i].astype(jnp.float32)
+        total = accs[s][lax.rem(i, p.slots)] + rcvs[s][layer, i].astype(jnp.float32)
         before = st[layer, own_rows, lanes].astype(jnp.float32)
         value = total * down_scale[layer : layer + 1, lanes] + RESIDUAL * before
         value = value.astype(jnp.bfloat16)
@@ -504,69 +608,31 @@
             gather1(a + 1, f).start()
         else:
             squares(1, chunk_lanes(f), i == 0)
+            product_stage(1, 3, up, i)
 
     def pipeline(stages, tasks):
-        count = p.n_chunks + len(stages) - 1
+        count = p.n_chunks + stages[-1][0]
 
         @pl.loop(0, count)
         def _(it):
-            for back in reversed(range(len(stages))):
-                i = it - back
+            for back, (lag, stage) in reversed(list(enumerate(stages))):
+                i = it - lag
 
                 @pl.when(jnp.logical_and(i >= 0, i < p.n_chunks))
                 def _():
-                    stages[back](i)
-
-            for index, task in enumerate(tasks):
-
-                @pl.when(it == 1 + index * (count - 2) // len(tasks))
+                    with jax.named_scope(f"stage#b={back}"):
+                        stage(i)
+
+            for when, task in tasks:
+
+                @pl.when(it == when)
                 def _():
                     task()
 
-    def pump(k):
-        for dz in far:
-            forward(k, dz)
-        if k + 2 < n_k:
-            forward(k + 2, 0)
-            forward(k + 2, 1)
-
-    for layer in range(p.layers):
-        last = layer + 1 == p.layers
-        k = 3 * layer
-        if layer:
-            for dz in far:
-                z_send(k + 2, dz).start()
-        pump(k)
-        product(layer, k, up)
-        pump(k + 1)
-        product(layer, k + 1, gate)
-        convolve(layer)
-        pump(k + 2)
-        stages = [functools.partial(down_stage, layer)]
-        stages += [functools.partial(reduce_stage, layer, s) for s in range(1, p.n_steps)]
-        stages += [functools.partial(last_stage, layer)]
-        tasks = []
-        if not last:
-            stages += [functools.partial(gather_stage, a) for a in range(p.n_steps)]
-            tasks = [
-                lambda k=k, dz=dz: z_send(k, dz).start() for k in (k + 3, k + 4) for dz in far
-            ]
-        pipeline(stages, tasks)
-
-        @pl.loop(0, p.n_chunks)
-        def _(i):
-            for s in range(p.n_steps):
-                reduce_copy(layer, s, i).wait_send()
-
-        @pl.when(following < p.groups)
-        def _():
-            halo_copy(layer, 0).wait_send()
-            halo_copy(layer, 1).wait_send()
-
     sources = [
         (pz, py)
+        for pz in range(0, p.n_z, 2)
         for py in range(p.n_y)
-        for pz in range(0, p.n_z, 2)
     ]
     n_out = p.n_steps - 1
 
@@ -588,29 +654,127 @@
             partner(p.n_steps - 1 - a),
         )
 
-    for index, (pz, py) in enumerate(sources):
+    def out_first(index):
+        pz, py = sources[index]
         for low in range(2):
             dev = flip(z - m + low, pz) * p.n_y + flip(y, py)
 
             @pl.when(dev != r)
             def _():
-                ref = obuf.at[at_rows(first_token(dev), p.own)]
-                copy(ref, ref, sem["o_s"].at[0, 0], sem["o_r"].at[dev], (r, j)).wait_recv()
+                with jax.named_scope(f"out0#i={index}"):
+                    ref = obuf.at[at_rows(first_token(dev), p.own)]
+                    copy(ref, ref, sem["o_s"].at[0, 0], sem["o_r"].at[dev], (r, j)).wait_recv()
 
         out_gather(index, 1).start()
+
+    def halo_done(layer):
+        @pl.when(following < p.groups)
+        def _():
+            halo_copy(layer, 0).wait_send()
+            halo_copy(layer, 1).wait_send()
+
+    def far_forward(k):
+        with jax.named_scope(f"far#k={k}"):
+            for dz in far:
+                forward(k, dz)
+
+    def near_forward(k):
+        with jax.named_scope(f"near#k={k}"):
+            forward(k, 1)
+
+    for layer in range(p.layers):
+        last = layer + 1 == p.layers
+        k = 3 * layer
+        if layer == 0:
+            far_send(3)
+            with jax.named_scope(f"up#l={layer}"):
+                product(layer, k, up)
+            far_forward(1)
+            near_forward(2)
+            forward(3, 0)
+        if layer:
+            far_forward(4)
+        with jax.named_scope(f"gate#l={layer}"):
+            product(layer, k + 1, gate)
+        with jax.named_scope(f"convolve#l={layer}"):
+            convolve(layer, lambda: None)
+        if layer == 0:
+
+            @pl.when(inner)
+            def _():
+                far_send(4)
+                far_send(5)
+
+        stages = [(0, functools.partial(down_stage, layer))]
+        lag = 1
+        for step in range(1, p.n_steps):
+            stages.append((lag, functools.partial(reduce_stage, layer, step)))
+            lag += 2
+        stages.append((lag, functools.partial(last_stage, layer)))
+        tasks = []
+        if not last:
+            for step in range(p.n_steps):
+                lag += 2 if step + 1 < p.n_steps else 1
+                stages.append((lag, functools.partial(gather_stage, step)))
+
+            def outer_send(k):
+                @pl.when(jnp.logical_not(inner))
+                def _():
+                    far_send(k)
+
+            tasks = [
+                (1, lambda: far_forward(2)),
+                (2, lambda: near_forward(3)),
+                (2, lambda: forward(4, 0)),
+                (3, lambda: near_forward(4)),
+                (3, lambda: forward(5, 0)),
+                (5, lambda: near_forward(5)),
+                (8, lambda: outer_send(4)),
+                (10, lambda: far_forward(3)),
+                (13, lambda: outer_send(5)),
+            ]
+        else:
+            tasks = [(3, lambda: far_forward(5))]
+            count = p.n_chunks + lag
+            early = [index for index in range(p.groups) if p.q == 1 and 2 * index + 4 + lag < count]
+            tasks += [
+                (2 * index + 4 + lag, functools.partial(out_first, index)) for index in early
+            ]
+        with jax.named_scope(f"down#l={layer}"):
+            pipeline(stages, tasks)
+
+        @pl.loop(0, p.n_chunks)
+        def _(i):
+            for s in range(p.n_steps):
+                reduce_copy(layer, s, i).wait_send()
+
+        if last:
+            halo_done(layer)
+
+    for index in range(len(sources)):
+        if index not in early:
+            out_first(index)
     for a in range(1, p.n_steps):
         for index in range(len(sources)):
             ref = out_rows(index, a, True)
-            copy(
-                ref, ref, sem["oa_s"].at[a - 1, index], sem["oa_r"].at[a - 1, index], (r, j)
-            ).wait_recv()
+            with jax.named_scope(f"out{a}#i={index}"):
+                copy(
+                    ref, ref, sem["oa_s"].at[a - 1, index], sem["oa_r"].at[a - 1, index], (r, j)
+                ).wait_recv()
             if a + 1 < p.n_steps:
                 out_gather(index, a + 1).start()
 
     result = pltpu.make_async_copy(obuf, out, sem["local"].at[0])
     result.start()
+    finish = jax.named_scope("finish")
+    finish.__enter__()
     for off in range(1, p.n_ra):
         token_send(off).wait_send()
+
+        @pl.when(group_of(flip(r, off)) > 0)
+        def _():
+            extra_send(off).wait_send()
+
     for k in range(n_k):
         for dz in range(1, p.n_z):
             z_send(k, dz).wait_send()
@@ -634,6 +798,7 @@
         for index in range(len(sources)):
             out_gather(index, a).wait_send()
     result.wait()
+    finish.__exit__(None, None, None)
 
 
 def per_device(
@@ -665,9 +830,11 @@
     in_vmem = pl.BlockSpec(memory_space=pltpu.VMEM)
     sems = {
         "stage": dma((2,)),
-        "local": dma((1,)),
+        "local": dma((2,)),
         "tok_s": dma((p.n_ra,)),
         "tok_r": dma((p.n_ra,)),
+        "toke_s": dma((p.n_ra,)),
+        "toke_r": dma((p.n_ra,)),
         "w": dma((n_k, p.n_ra)),
         "z": dma((n_k, p.n_z)),
         "y": dma((n_k, p.n_z, p.n_y)),
@@ -688,7 +855,7 @@
     n_s = p.n_steps
 
     def body(*refs):
-        head, rest = refs[:11 + 12], refs[11 + 12 :]
+        head, rest = refs[: 11 + 17], refs[11 + 17 :]
         accs, snds, rcvs = rest[:n_s], rest[n_s : 2 * n_s], rest[2 * n_s : 3 * n_s]
         kernel(p, *head, accs, snds, rcvs, dict(zip(names, rest[3 * n_s :])))
 
@@ -706,12 +873,17 @@
             pltpu.VMEM((p.edge + p.group_tokens, p.half), f32),
             pltpu.VMEM((p.group_tokens, p.half), bf16),
             pltpu.VMEM((p.n_ra, p.own, rows), bf16),
+            pltpu.VMEM((p.n_ra, p.extra, rows), bf16),
+            pltpu.VMEM((p.extra, p.features), bf16),
+            pltpu.VMEM((p.extra, p.half), f32),
+            pltpu.VMEM((p.extra, p.half), f32),
+            pltpu.VMEM((p.extra, 128), f32),
             pltpu.VMEM((p.group_tokens, 128), f32),
             pltpu.VMEM((layers, 2, p.edge, p.half), f32),
             pltpu.VMEM((p.length, rows), bf16),
             pltpu.VMEM((p.n_chunks, p.q, p.own, rows), bf16),
         ]
-        + [pltpu.VMEM((size, p.chunk), f32) for size in p.sizes]
+        + [pltpu.VMEM((p.slots, size, p.chunk), f32) for size in p.sizes]
         + [pltpu.VMEM((p.n_chunks, size, p.chunk), bf16) for size in p.sizes]
         + [pltpu.VMEM((layers, p.n_chunks, size, p.chunk), bf16) for size in p.sizes]
         + [sems[name] for name in names],
@@ -727,8 +899,8 @@
         norm_gain,
         up_scale,
         gate_scale,
-        up_taps,
-        gate_taps,
+        jnp.swapaxes(up_taps, 0, 1),
+        jnp.swapaxes(gate_taps, 0, 1),
         down_scale,
     )
     return turned.T

time: 370 us -> 302 us (0.82); the launches traced: 370 us -> 298 us
  Pallas kernels: 359 us -> 289 us
    pallas_call x1, Pallas kernels: 359 us -> 289 us  [per_device(): pl.pallas_call(body, out_shape=jax.ShapeDtypeStruct((p.length, rows), bf1...]
where the time goes in v1:
time: 302 us; the launch traced here: 298 us
  Pallas kernels  289 us (96%)
  local copies, waits for them, and re-layouts  8.14 us (3%)
    pallas_call x1, Pallas kernels, per_device(): pl.pallas_call(body, out_shape=jax.ShapeDtypeStruct((p.length, rows), bf1...  289 us

profile of v1, /device:TPU:17, one launch (start us, length us, event | category | flops | bytes accessed | tf_op | source)
XLA Modules:
  0.0 297.6 jit_solution(16598774892808194257)
XLA Ops:
  0.0 4.1 %copy.11 = bf16[256,4096]{0,1:T(8,128)(2,1)} copy(bf16[256,4096]{1,0:T(8,128)(2,1)} %param.10) | data formatting | bytes 4194304 | tf_op args[0]
  4.1 289.5 %layers.1 = bf16[4096,256]{1,0:T(8,128)(2,1)} custom-call(bf16[4096,256]{1,0:T(8,128)(2,1)} %bitcast.5, f32[2,256,1536]{2,1,0:T(8,128)} %refs_1_.1, f32[2,256,1536]{2,1,0:T(8,128)} %refs_2_.1, f32[2,256,1536]{2,1,0:T(8,128)} %refs_3_.1, f32[2,2048]{1,0:T(2,128)} %refs_4_.1, f32[2,1536]{1,0:T(2,128)} %refs_5_.1, f32[2,1536]{1,0:T(2,128)} %refs_6_.1, ...), custom_call_target="tpu_custom_call" | custom-call | tf_op jit(solution)/shard_map/layers/pallas_call | solution.py:862
  293.6 4.1 %copy.12 = bf16[256,4096]{1,0:T(8,128)(2,1)} copy(bf16[256,4096]{0,1:T(8,128)(2,1)} %bitcast.4) | data formatting | bytes 4194304 | tf_op jit(solution)/shard_map/transpose | solution.py:906

commit v2 on v1

--- a/solution.py
+++ b/solution.py
@@ -85,6 +85,7 @@
     gate_e,
     sq_e,
     sq,
+    tail,
     halo,
     obuf,
     ost,
@@ -232,6 +233,10 @@
         return jnp.logical_and(plane > 0, plane < p.n_z - 1)
 
     def far_send(k):
+        if k >= 3:
+            for dz in far:
+                z_send(k, dz).start()
+            return
         for wanted in (True, False):
             for dz in far:
 
@@ -415,10 +420,11 @@
                 to = (up_e, gate_e)[k % 3]
                 to[...] = term if first else to[...] + term
 
-    def product(layer, k, dst):
-        product_chunk(layer, k, dst, 0, True)
-
-        @pl.loop(1, p.n_chunks)
+    def product(layer, k, dst, start, stop):
+        if start == 0:
+            product_chunk(layer, k, dst, 0, True)
+
+        @pl.loop(max(start, 1), stop)
         def _(i):
             product_chunk(layer, k, dst, i, False)
 
@@ -436,34 +442,57 @@
     following_dev = (lax.div(following, p.n_y) * 2 + m) * p.n_y + lax.rem(following, p.n_y)
 
     def halo_copy(layer, which):
-        source = (up, gate)[which]
         return copy(
-            source.at[pl.ds(p.group_tokens, p.edge)],
+            tail.at[layer, which],
             halo.at[layer, which],
             sem["h_s"].at[layer, which],
             sem["h_r"].at[layer, which],
             (following_dev, j),
         )
 
-    def convolve(layer, between=None):
-        scale_u = up_scale[layer : layer + 1, own_half]
-        scale_g = gate_scale[layer : layer + 1, own_half]
-
-        @pl.loop(0, p.group_tokens // fine)
-        def _(t):
-            total = jnp.sum(sq[at_rows(t * fine, fine), :], axis=1, keepdims=True)
-            inverse = lax.rsqrt(total * (1.0 / p.features) + EPS)
-            rows = pl.ds(pl.multiple_of(p.edge + t * fine, 8), fine)
-            up[rows, :] = up[rows, :] * inverse * scale_u
-            gate[rows, :] = gate[rows, :] * inverse * scale_g
-
+    def inverse_of(squares_sum):
+        total = jnp.sum(squares_sum, axis=1, keepdims=True)
+        return lax.rsqrt(total * (1.0 / p.features) + EPS)
+
+    def convolve(layer, between):
         if layer:
+            inverse = inverse_of(sq[p.group_tokens - p.edge : p.group_tokens, :])
+            ends = slice(p.group_tokens, p.group_tokens + p.edge)
+            tail[layer, 0] = up[ends, :] * inverse
+            tail[layer, 1] = gate[ends, :] * inverse
 
             @pl.when(following < p.groups)
             def _():
                 halo_copy(layer, 0).start()
                 halo_copy(layer, 1).start()
 
+        taps_u = up_taps[:, layer, own_half] * up_scale[layer : layer + 1, own_half]
+        taps_g = gate_taps[:, layer, own_half] * gate_scale[layer : layer + 1, own_half]
+        low = p.edge + 1 - p.width
+
+        def taps_over(values, taps):
+            total = taps[0:1] * values[low : low + fine]
+            for c in range(1, p.width):
+                total = total + taps[c : c + 1] * values[low + c : low + c + fine]
+            return total
+
+        def finish_tile(up_values, gate_values, t):
+            conv_gate = taps_over(gate_values, taps_g)
+            conv_up = taps_over(up_values, taps_u)
+            value = conv_gate / (1.0 + jnp.exp(-conv_gate)) * conv_up
+            hid[at_rows(t * fine, fine), :] = value.astype(jnp.bfloat16)
+
+        tiles = p.group_tokens // fine
+
+        @pl.loop(0, tiles - 1)
+        def _(step):
+            t = tiles - 1 - step
+            before = pl.ds(pl.multiple_of(t * fine - p.edge, 8), fine + p.edge)
+            inverse = inverse_of(sq[before, :])
+            rows = pl.ds(pl.multiple_of(t * fine, 8), fine + p.edge)
+            finish_tile(up[rows, :] * inverse, gate[rows, :] * inverse, t)
+
+        if layer:
             between()
 
         @pl.when(group > 0)
@@ -479,35 +508,22 @@
                     ).wait_recv()
                     dst[0 : p.edge, :] = halo[layer, which]
             else:
-                total = jnp.sum(sq_e[...], axis=1, keepdims=True)
-                inverse = lax.rsqrt(total * (1.0 / p.features) + EPS)
-                up_values = up_e[...] * inverse * scale_u
-                gate_values = gate_e[...] * inverse * scale_g
-                up[0 : p.edge, :] = up_values[p.extra - p.edge :]
-                gate[0 : p.edge, :] = gate_values[p.extra - p.edge :]
+                inverse = inverse_of(sq_e[...])[p.extra - p.edge :]
+                up[0 : p.edge, :] = up_e[p.extra - p.edge :, :] * inverse
+                gate[0 : p.edge, :] = gate_e[p.extra - p.edge :, :] * inverse
 
         @pl.when(group == 0)
         def _():
             up[0 : p.edge, :] = jnp.zeros((p.edge, p.half), jnp.float32)
             gate[0 : p.edge, :] = jnp.zeros((p.edge, p.half), jnp.float32)
 
-        taps_u = up_taps[:, layer, own_half]
-        taps_g = gate_taps[:, layer, own_half]
-
-        def taps_over(ref, taps, t):
-            values = ref[pl.ds(pl.multiple_of(t * fine, 8), fine + p.edge), :]
-            low = p.edge + 1 - p.width
-            total = taps[0:1] * values[low : low + fine]
-            for c in range(1, p.width):
-                total = total + taps[c : c + 1] * values[low + c : low + c + fine]
-            return total
-
-        @pl.loop(0, p.group_tokens // fine)
-        def _(t):
-            conv_gate = taps_over(gate, taps_g, t)
-            conv_up = taps_over(up, taps_u, t)
-            value = conv_gate / (1.0 + jnp.exp(-conv_gate)) * conv_up
-            hid[at_rows(t * fine, fine), :] = value.astype(jnp.bfloat16)
+        inverse = inverse_of(sq[0:fine, :])
+        first = slice(p.edge, p.edge + fine)
+        finish_tile(
+            jnp.concatenate([up[0 : p.edge, :], up[first, :] * inverse], axis=0),
+            jnp.concatenate([gate[0 : p.edge, :], gate[first, :] * inverse], axis=0),
+            0,
+        )
 
     def reduce_copy(layer, s, i):
         return copy(
@@ -552,10 +568,10 @@
     def reduce_stage(layer, s, i):
         reduce_wait(layer, s - 1, i)
         size = p.sizes[s]
+        slot = lax.rem(i, p.slots)
         give_rows = at_rows((1 - mine[s]) * size, size)
         keep_rows = at_rows(mine[s] * size, size)
         arrived = rcvs[s - 1][layer, i, give_rows, :].astype(jnp.float32)
-        slot = lax.rem(i, p.slots)
         snds[s][i] = (accs[s - 1][slot, give_rows, :] + arrived).astype(jnp.bfloat16)
         arrived = rcvs[s - 1][layer, i, keep_rows, :].astype(jnp.float32)
         accs[s][slot] = accs[s - 1][slot, keep_rows, :] + arrived
@@ -673,9 +689,9 @@
             halo_copy(layer, 0).wait_send()
             halo_copy(layer, 1).wait_send()
 
-    def far_forward(k):
+    def far_forward(k, part=slice(None)):
         with jax.named_scope(f"far#k={k}"):
-            for dz in far:
+            for dz in far[part]:
                 forward(k, dz)
 
     def near_forward(k):
@@ -688,16 +704,19 @@
         if layer == 0:
             far_send(3)
             with jax.named_scope(f"up#l={layer}"):
-                product(layer, k, up)
+                product(layer, k, up, 0, p.n_chunks)
             far_forward(1)
             near_forward(2)
             forward(3, 0)
-        if layer:
-            far_forward(4)
         with jax.named_scope(f"gate#l={layer}"):
-            product(layer, k + 1, gate)
+            if layer:
+                product(layer, k + 1, gate, 0, p.n_chunks - 2)
+                far_forward(5, slice(1))
+                product(layer, k + 1, gate, p.n_chunks - 2, p.n_chunks)
+            else:
+                product(layer, k + 1, gate, 0, p.n_chunks)
         with jax.named_scope(f"convolve#l={layer}"):
-            convolve(layer, lambda: None)
+            convolve(layer, lambda: far_forward(5, slice(1, None)))
         if layer == 0:
 
             @pl.when(inner)
@@ -730,11 +749,13 @@
                 (3, lambda: forward(5, 0)),
                 (5, lambda: near_forward(5)),
                 (8, lambda: outer_send(4)),
-                (10, lambda: far_forward(3)),
-                (13, lambda: outer_send(5)),
+                (9, lambda: far_forward(3, slice(1))),
+                (10, lambda: far_forward(3, slice(1, None))),
+                (12, lambda: outer_send(5)),
+                (13, lambda: far_forward(4, slice(1))),
+                (15, lambda: far_forward(4, slice(1, None))),
             ]
         else:
-            tasks = [(3, lambda: far_forward(5))]
             count = p.n_chunks + lag
             early = [index for index in range(p.groups) if p.q == 1 and 2 * index + 4 + lag < count]
             tasks += [
@@ -855,7 +876,7 @@
     n_s = p.n_steps
 
     def body(*refs):
-        head, rest = refs[: 11 + 17], refs[11 + 17 :]
+        head, rest = refs[: 11 + 18], refs[11 + 18 :]
         accs, snds, rcvs = rest[:n_s], rest[n_s : 2 * n_s], rest[2 * n_s : 3 * n_s]
         kernel(p, *head, accs, snds, rcvs, dict(zip(names, rest[3 * n_s :])))
 
@@ -879,6 +900,7 @@
             pltpu.VMEM((p.extra, p.half), f32),
             pltpu.VMEM((p.extra, 128), f32),
             pltpu.VMEM((p.group_tokens, 128), f32),
+            pltpu.VMEM((layers, 2, p.edge, p.half), f32),
             pltpu.VMEM((layers, 2, p.edge, p.half), f32),
             pltpu.VMEM((p.length, rows), bf16),
             pltpu.VMEM((p.n_chunks, p.q, p.own, rows), bf16),

time: 302 us -> 285 us (0.944)
  Pallas kernels: 289 us -> 274 us
    pallas_call x1, Pallas kernels: 289 us -> 274 us  [per_device(): pl.pallas_call(body, out_shape=jax.ShapeDtypeStruct((p.length, rows), bf1...]
where the time goes in v2:
time: 285 us; the launch traced here: 282 us
  Pallas kernels  274 us (96%)
  local copies, waits for them, and re-layouts  8.14 us (3%)
    pallas_call x1, Pallas kernels, per_device(): pl.pallas_call(body, out_shape=jax.ShapeDtypeStruct((p.length, rows), bf1...  274 us

profile of v2, /device:TPU:17, one launch (start us, length us, event | category | flops | bytes accessed | tf_op | source)
XLA Modules:
  0.0 282.0 jit_solution(9186641522239553453)
XLA Ops:
  0.0 4.1 %copy.11 = bf16[256,4096]{0,1:T(8,128)(2,1)} copy(bf16[256,4096]{1,0:T(8,128)(2,1)} %param.10) | data formatting | bytes 4194304 | tf_op args[0]
  4.1 273.9 %layers.1 = bf16[4096,256]{1,0:T(8,128)(2,1)} custom-call(bf16[4096,256]{1,0:T(8,128)(2,1)} %bitcast.5, f32[2,256,1536]{2,1,0:T(8,128)} %refs_1_.1, f32[2,256,1536]{2,1,0:T(8,128)} %refs_2_.1, f32[2,256,1536]{2,1,0:T(8,128)} %refs_3_.1, f32[2,2048]{1,0:T(2,128)} %refs_4_.1, f32[2,1536]{1,0:T(2,128)} %refs_5_.1, f32[2,1536]{1,0:T(2,128)} %refs_6_.1, ...), custom_call_target="tpu_custom_call" | custom-call | tf_op jit(solution)/shard_map/layers/pallas_call | solution.py:883
  278.0 4.1 %copy.12 = bf16[256,4096]{1,0:T(8,128)(2,1)} copy(bf16[256,4096]{0,1:T(8,128)(2,1)} %bitcast.4) | data formatting | bytes 4194304 | tf_op jit(solution)/shard_map/transpose | solution.py:928

commit v3 on v2

--- a/solution.py
+++ b/solution.py
@@ -324,6 +324,7 @@
     far_send(0)
     forward(2, 0)
     convert(4)
+    forward(3, 0)
     convert(5)
     for a in range(p.n_steps):
         with jax.named_scope(f"gather0#a={a}"):
@@ -492,6 +493,7 @@
             rows = pl.ds(pl.multiple_of(t * fine, 8), fine + p.edge)
             finish_tile(up[rows, :] * inverse, gate[rows, :] * inverse, t)
 
+
         if layer:
             between()
 
@@ -670,6 +672,12 @@
             partner(p.n_steps - 1 - a),
         )
 
+    def out_store(index):
+        pz, py = sources[index]
+        dev = flip(z, pz) * p.n_y + flip(y, py)
+        rows = at_rows(group_of(dev) * p.group_tokens, p.group_tokens)
+        return pltpu.make_async_copy(obuf.at[rows], out.at[rows], sem["store"].at[index])
+
     def out_first(index):
         pz, py = sources[index]
         for low in range(2):
@@ -707,7 +715,6 @@
                 product(layer, k, up, 0, p.n_chunks)
             far_forward(1)
             near_forward(2)
-            forward(3, 0)
         with jax.named_scope(f"gate#l={layer}"):
             if layer:
                 product(layer, k + 1, gate, 0, p.n_chunks - 2)
@@ -784,9 +791,9 @@
                 ).wait_recv()
             if a + 1 < p.n_steps:
                 out_gather(index, a + 1).start()
-
-    result = pltpu.make_async_copy(obuf, out, sem["local"].at[0])
-    result.start()
+            else:
+                out_store(index).start()
+
     finish = jax.named_scope("finish")
     finish.__enter__()
     for off in range(1, p.n_ra):
@@ -818,7 +825,8 @@
     for a in range(1, p.n_steps):
         for index in range(len(sources)):
             out_gather(index, a).wait_send()
-    result.wait()
+    for index in range(len(sources)):
+        out_store(index).wait()
     finish.__exit__(None, None, None)
 
 
@@ -852,6 +860,7 @@
     sems = {
         "stage": dma((2,)),
         "local": dma((2,)),
+        "store": dma((p.groups,)),
         "tok_s": dma((p.n_ra,)),
         "tok_r": dma((p.n_ra,)),
         "toke_s": dma((p.n_ra,)),

time: 285 us -> 282 us (0.989)
  Pallas kernels: 274 us -> 270 us
    pallas_call x1, Pallas kernels: 274 us -> 270 us  [per_device(): pl.pallas_call(body, out_shape=jax.ShapeDtypeStruct((p.length, rows), bf1...]
where the time goes in v3:
time: 282 us; the launch traced here: 278 us
  Pallas kernels  270 us (96%)
  local copies, waits for them, and re-layouts  8.14 us (3%)
    pallas_call x1, Pallas kernels, per_device(): pl.pallas_call(body, out_shape=jax.ShapeDtypeStruct((p.length, rows), bf1...  270 us

profile of v3, /device:TPU:17, one launch (start us, length us, event | category | flops | bytes accessed | tf_op | source)
XLA Modules:
  0.0 278.0 jit_solution(11662108237035611231)
XLA Ops:
  0.0 4.1 %copy.11 = bf16[256,4096]{0,1:T(8,128)(2,1)} copy(bf16[256,4096]{1,0:T(8,128)(2,1)} %param.10) | data formatting | bytes 4194304 | tf_op args[0]
  4.1 269.8 %layers.1 = bf16[4096,256]{1,0:T(8,128)(2,1)} custom-call(bf16[4096,256]{1,0:T(8,128)(2,1)} %bitcast.5, f32[2,256,1536]{2,1,0:T(8,128)} %refs_1_.1, f32[2,256,1536]{2,1,0:T(8,128)} %refs_2_.1, f32[2,256,1536]{2,1,0:T(8,128)} %refs_3_.1, f32[2,2048]{1,0:T(2,128)} %refs_4_.1, f32[2,1536]{1,0:T(2,128)} %refs_5_.1, f32[2,1536]{1,0:T(2,128)} %refs_6_.1, ...), custom_call_target="tpu_custom_call" | custom-call | tf_op jit(solution)/shard_map/layers/pallas_call | solution.py:892
  273.9 4.1 %copy.12 = bf16[256,4096]{1,0:T(8,128)(2,1)} copy(bf16[256,4096]{0,1:T(8,128)(2,1)} %bitcast.4) | data formatting | bytes 4194304 | tf_op jit(solution)/shard_map/transpose | solution.py:937
